TPU v7x, 512 devices: a 4x2x32 block of a 4x8x32 slice. The times are simulated.
512 devices in a mesh: grp: 2 (over y), ep: 64 (over z, core), tp: 4 (over x).
Axes of the slice: x: 4, y: 2, z: 32, core: 2. Of those that a mesh axis runs over, the one named last changes fastest.
The devices are a block of a 4x8x32 slice.
Arguments:
- tokens: bfloat16 [24576, 2048], P(('grp', 'ep')), parts along dimension 0, may hold values from -6 to 6
- norm_gain: float32 [2048], replicated, may hold values from 0.1 to 1.9
- w_gate: bfloat16 [64, 2048, 1024], P('ep', None, 'tp'), may hold values from -0.3125 to 0.3125
- w_up: bfloat16 [64, 2048, 1024], P('ep', None, 'tp'), may hold values from -0.3125 to 0.3125
- w_down: bfloat16 [64, 1024, 2048], P('ep', 'tp'), may hold values from -0.09375 to 0.09375
- expert_ids: int32 [24576, 4], P(('grp', 'ep')), parts along dimension 0, may hold values from 0 to 63, all different within a row; in each aligned block of 192 rows (0 to 191, 192 to 383, ...) at most 16 rows name the same one
- gate_weights: float32 [24576, 4], P(('grp', 'ep')), parts along dimension 0, may hold values from 0.1 to 1
Outputs:
- mixed: bfloat16 [24576, 2048], P(('grp', 'ep'), 'tp'), parts along dimension 0
There are 2 independent parts, one for each index of `grp`. A program takes and returns all parts, laid end to end along the dimension named above; an argument that names none is the same for every part. Nothing has to cross between parts.
Inputs may be any that keep to these rules, and one draw needn't show every extreme that they name: `expert_ids`: each row names 4 different experts; among the rows of one index of ep, no expert is named by more than 16 rows, a bound that some block reaches.
All inputs are finite; a program needn't handle non-finite values.
Results may differ from a plain program's by a relative error of at most 0.012.
Values may be sent and summed in bfloat16 or wider, within the bound.
A program may use at most 64 MiB of HBM per device.

v0:
```python
import jax
import jax.numpy as jnp
from jax import lax
from jax.sharding import Mesh
from jax.sharding import PartitionSpec as P

EP = ("ep_0", "ep_1")
GRP_EP = ("grp", "ep_0", "ep_1")
epsilon = 1e-06
clamp_limit = 7.0
swish_alpha = 1.702


def cut_along(value, dim, devices):
    before, after = (value.shape[:dim], value.shape[dim + 1 :])
    return jnp.moveaxis(value.reshape(*before, devices, -1, *after), dim, 0)


def laid_out(blocks, dim):
    blocks = jnp.moveaxis(blocks, 0, dim)
    shape = blocks.shape
    return blocks.reshape(*shape[:dim], shape[dim] * shape[dim + 1], *shape[dim + 2 :])


def turned_blocks(blocks, axes, turns):
    inside = blocks.shape[1:]
    whole = blocks.reshape(*(lax.axis_size(a) for a in axes), *inside)
    for k in turns:
        whole = lax.all_to_all(whole, axes[k], k, k, tiled=True)
    return whole.reshape(-1, *inside)


def exchange_by_chip(value, groups, turns, split_dim, concat_dim):
    devices = lax.axis_size(groups[0]) * lax.axis_size(groups[1])
    blocks = cut_along(value, split_dim, devices)
    return laid_out(turned_blocks(blocks, groups, turns), concat_dim)


def sent_and_summed(value, axis, dim):
    blocks = cut_along(value, dim, lax.axis_size(axis))
    arrived = lax.all_to_all(blocks, axis, split_axis=0, concat_axis=0, tiled=True)
    return arrived.astype(jnp.float32).sum(axis=0)


def rms_norm(tokens, norm_gain):
    widened = tokens.astype(jnp.float32)
    scaled = widened * lax.rsqrt(jnp.mean(widened * widened, axis=-1, keepdims=True) + epsilon)
    return (scaled * norm_gain).astype(jnp.bfloat16)


def body(tokens, norm_gain, w_gate, w_up, w_down, expert_ids, gate_weights):
    tok_rows, model_width = tokens.shape
    top_count = expert_ids.shape[1]
    ep_count = lax.axis_size(EP)
    tp_count = lax.axis_size("tp")
    local_experts = w_gate.shape[0]
    experts_all = local_experts * ep_count
    capacity = min(tok_rows, tok_rows * top_count * 4 // (3 * experts_all))
    normed = rms_norm(tokens, norm_gain)
    flat_ids = expert_ids.reshape(-1)
    onehot = (flat_ids[:, None] == jnp.arange(experts_all, dtype=jnp.int32)[None, :]).astype(
        jnp.int32
    )
    before = jnp.cumsum(onehot, axis=0) - onehot
    slot_index = jnp.sum(before * onehot, axis=1)
    dest_row = flat_ids * capacity + slot_index
    owner_tok = jnp.arange(tok_rows * top_count, dtype=jnp.int32) // top_count
    slot_table = (
        jnp.full((experts_all * capacity,), tok_rows, jnp.int32).at[dest_row].set(owner_tok)
    )
    padded = jnp.concatenate([normed, jnp.zeros((1, model_width), jnp.bfloat16)], axis=0)
    send_buffer = padded[slot_table].reshape(experts_all, capacity, model_width)
    col_share = model_width // tp_count
    col_part = lax.dynamic_slice_in_dim(send_buffer, lax.axis_index("tp") * col_share, col_share, 2)
    received = exchange_by_chip(col_part, ("ep_0", "ep_1"), (1, 0), 0, 0)
    received = lax.all_gather(received, "tp", axis=2, tiled=True)
    expert_rows = received.reshape(ep_count, local_experts, capacity, model_width)
    gate_pre = jnp.einsum("sjcd,jdf->sjcf", expert_rows, w_gate, preferred_element_type=jnp.float32)
    up_pre = jnp.einsum("sjcd,jdf->sjcf", expert_rows, w_up, preferred_element_type=jnp.float32)
    gated = jnp.minimum(gate_pre, clamp_limit)
    linear = jnp.clip(up_pre, -clamp_limit, clamp_limit)
    activated = (gated * jax.nn.sigmoid(swish_alpha * gated) * (linear + 1.0)).astype(jnp.bfloat16)
    partial_value = jnp.einsum(
        "sjcf,jfd->sjcd", activated, w_down, preferred_element_type=jnp.float32
    ).astype(jnp.bfloat16)
    summed = sent_and_summed(partial_value, "tp", 3).astype(jnp.bfloat16)
    returned = exchange_by_chip(summed, ("ep_0", "ep_1"), (1, 0), 0, 0)
    returned = returned.reshape(experts_all * capacity, returned.shape[3])
    picked = returned[dest_row].reshape(tok_rows, top_count, returned.shape[1]).astype(jnp.float32)
    return jnp.sum(picked * gate_weights[:, :, None], axis=1).astype(jnp.bfloat16)


def solution(mesh):
    torus = Mesh(
        mesh.devices.reshape(mesh.shape["grp"], 32, 2, mesh.shape["tp"]),
        ("grp", "ep_0", "ep_1", "tp"),
    )
    return jax.shard_map(
        body,
        mesh=torus,
        in_specs=(
            P(GRP_EP, None),
            P(),
            P(EP, None, "tp"),
            P(EP, None, "tp"),
            P(EP, "tp", None),
            P(GRP_EP, None),
            P(GRP_EP, None),
        ),
        out_specs=P(GRP_EP, "tp"),
        check_vma=False,
    )
```

profile of v0, /device:TPU:33, one launch (start us, length us, event | category | flops | bytes accessed | tf_op | source)
XLA Modules:
  0.0 449.6 jit_solution(9208010235505050856)
XLA Ops:
  6.5 0.0 copy-start
  6.6 0.0 all-gather.2.cloned.1.call-start
  6.6 0.9 copy.23
  7.4 0.1 eq.29
  7.6 0.1 eq.25
  7.7 0.7 broadcast_multiply_fusion
  8.4 1.8 reduce-window.6
  10.2 0.3 slice_reduce_fusion
  10.5 0.1 copy.22
  10.6 0.1 mul.68
  10.7 0.1 fusion.26
  10.9 3.4 scatter_custom_fusion
  14.3 1.4 fusion
  15.7 1.4 fusion.2
  17.1 0.1 concatenate.3
  17.2 6.0 %gather_fusion = bf16[1024,2048]{1,0:T(8,128)(2,1)} fusion(bf16[193,2048]{1,0:T(8,128)(2,1)S(1)} %concatenate.3, s32[1024]{0:T(1024)S(1)} %fusion.30), kind=kCustom, calls=%fused_computation | custom fusion | bytes 8392704 | tf_op jit(solution)/shard_map/gather | solution.py:72
  23.2 1.3 constant_dynamic-slice_fusion
  24.5 0.1 copy.26
  24.6 0.0 copy-start.2
  24.6 45.8 %all_to_all.25 = bf16[32,2,1,16,512]{4,3,0,2,1:T(8,128)(2,1)S(1)} all-to-all(bf16[32,2,1,16,512]{4,3,0,2,1:T(8,128)(2,1)S(1)} %copy.26), channel_id=1, replica_groups=mesh['grp'=2,'ep_0'=32,'ep_1'=2,'tp'=4] {'ep_1'}, dimensions={1} | all-to-all | bytes 2097152 | tf_op jit(solution)/shard_map/all_to_all | solution.py:29
  70.4 0.1 copy.27
  70.5 110.0 %all_to_all.26 = bf16[32,2,1,16,512]{4,3,1,2,0:T(8,128)(2,1)} all-to-all(bf16[32,2,1,16,512]{4,3,1,2,0:T(8,128)(2,1)S(1)} %copy.27), channel_id=1, replica_groups=mesh['grp'=2,'ep_0'=32,'ep_1'=2,'tp'=4] {'ep_0'}, dimensions={0} | all-to-all | bytes 2097152 | tf_op jit(solution)/shard_map/all_to_all | solution.py:29
  180.5 0.0 copy-start.3
  180.5 0.1 all-gather.2.cloned.1.call-update
  180.5 51.5 %all-gather.2.cloned.1.call-done = bf16[64,16,2048]{2,1,0:T(8,128)(2,1)} async-done(((bf16[64,16,512]{2,1,0:T(8,128)(2,1)}), bf16[64,16,2048]{2,1,0:T(8,128)(2,1)}) %all-gather.2.cloned.1.call-update) | async-done | bytes 4194320 | tf_op jit(solution)/shard_map/all_gather | solution.py:76
  232.1 0.0 copy-done.2
  232.1 4.5 %fusion.3 = f32[64,1,16,256]{3,2,0,1:T(8,128)} fusion(bf16[64,16,2048]{2,1,0:T(8,128)(2,1)} %all-gather.2.cloned.1.call-done, bf16[1,2048,256]{2,1,0:T(8,128)(2,1)S(1)} %copy-done.2), kind=kOutput, calls=%fused_computation.12 | convolution fusion | flops 1074003968 | bytes 6291456 | tf_op jit(solution)/shard_map/sjcd,jdf->sjcf/dot_general | solution.py:78
  236.6 0.0 copy-done
  236.6 0.0 copy-done.3
  236.6 8.9 %convolution_convert_fusion = bf16[64,16,2048]{2,1,0:T(8,128)(2,1)} fusion(bf16[64,16,2048]{2,1,0:T(8,128)(2,1)} %all-gather.2.cloned.1.call-done, bf16[1,256,2048]{2,1,0:T(8,128)(2,1)S(1)} %copy-done, bf16[1,2048,256]{2,1,0:T(8,128)(2,1)S(1)} %copy-done.3, f32[64,1,16,256]{3,2,0,1:T(8,128)} %fusion.3), kind=kOutput, calls=%fused_computation.4 | convolution fusion | flops 2151940096 | bytes 11534336 | tf_op jit(solution)/shard_map/sjcf,jfd->sjcd/dot_general | solution.py:83
  245.4 2.8 copy.36
  248.3 51.3 %all_to_all.27 = bf16[4,64,1,16,512]{4,3,1,2,0:T(8,128)(2,1)} all-to-all(bf16[4,64,1,16,512]{4,3,1,2,0:T(8,128)(2,1)S(1)} %bitcast.77), channel_id=1, replica_groups=mesh['grp'=2,'ep_0'=32,'ep_1'=2,'tp'=4] {'tp'}, dimensions={0} | all-to-all | bytes 8388608 | tf_op jit(solution)/shard_map/all_to_all | solution.py:41
  299.6 3.3 reduce_sum.44
  302.9 0.0 copy-start.1
  302.9 0.1 copy.29
  303.0 6.1 %all_to_all.28 = bf16[32,2,1,1,16,512]{5,4,0,3,2,1:T(8,128)(2,1)S(1)} all-to-all(bf16[32,2,1,1,16,512]{5,4,0,3,2,1:T(8,128)(2,1)S(1)} %copy.29), channel_id=1, replica_groups=mesh['grp'=2,'ep_0'=32,'ep_1'=2,'tp'=4] {'ep_1'}, dimensions={1} | all-to-all | bytes 2097152 | tf_op jit(solution)/shard_map/all_to_all | solution.py:29
  309.1 1.1 copy.30
  310.2 23.4 %all-to-all-start.4 = ((bf16[32,2,1,1,16,512]{5,4,1,3,2,0:T(8,128)(2,1)}), bf16[32,2,1,1,16,512]{5,4,1,3,2,0:T(8,128)(2,1)S(1)}, u32[]{:S(2)}, u32[]{:S(2)}) async-start(bf16[32,2,1,1,16,512]{5,4,1,3,2,0:T(8,128)(2,1)} %copy.30), calls=%async_computation.4 | async-start | bytes 2097152 | tf_op jit(solution)/shard_map/all_to_all | solution.py:29
  333.6 0.0 copy-done.1
  333.6 0.1 copy.31
  333.7 104.2 %all-to-all-done.4 = bf16[32,2,1,1,16,512]{5,4,1,3,2,0:T(8,128)(2,1)S(1)} async-done(((bf16[32,2,1,1,16,512]{5,4,1,3,2,0:T(8,128)(2,1)}), bf16[32,2,1,1,16,512]{5,4,1,3,2,0:T(8,128)(2,1)S(1)}, u32[]{:S(2)}, u32[]{:S(2)}) %all-to-all-start.4) | async-done | bytes 1048608 | tf_op jit(solution)/shard_map/all_to_all | solution.py:29
  437.9 2.7 gather_fusion.1
  440.6 0.5 reshape.102
  441.1 1.7 multiply_reduce_fusion
  (7 shorter events, 0.1 us)
Async XLA Ops:
  6.5 230.0 %copy-start = (bf16[1,256,2048]{2,1,0:T(8,128)(2,1)S(1)}, bf16[1,256,2048]{2,1,0:T(8,128)(2,1)}, u32[]{:S(2)}) copy-start(bf16[1,256,2048]{2,1,0:T(8,128)(2,1)} %param.11) | copy-start | bytes 3145732
  6.6 225.5 %all-gather.2.cloned.1.call-start = ((), (), s32[]{:S(2)}) async-start(), calls=%async_computation.5 | async-start | bytes 5242880 | tf_op jit(solution)/shard_map/all_gather | solution.py:76
  24.6 207.5 %copy-start.2 = (bf16[1,2048,256]{2,1,0:T(8,128)(2,1)S(1)}, bf16[1,2048,256]{2,1,0:T(8,128)(2,1)}, u32[]{:S(2)}) copy-start(bf16[1,2048,256]{2,1,0:T(8,128)(2,1)} %param.9) | copy-start | bytes 3145732
  180.5 56.1 %copy-start.3 = (bf16[1,2048,256]{2,1,0:T(8,128)(2,1)S(1)}, bf16[1,2048,256]{2,1,0:T(8,128)(2,1)}, u32[]{:S(2)}) copy-start(bf16[1,2048,256]{2,1,0:T(8,128)(2,1)} %param.10) | copy-start | bytes 3145732
  302.9 30.7 %copy-start.1 = (f32[192,4]{0,1:T(4,128)S(1)}, f32[192,4]{0,1:T(4,128)}, u32[]{:S(2)}) copy-start(f32[192,4]{0,1:T(4,128)} %param.13) | copy-start | bytes 9220
  310.2 127.7 %all-to-all-start.4 = ((bf16[32,2,1,1,16,512]{5,4,1,3,2,0:T(8,128)(2,1)}), bf16[32,2,1,1,16,512]{5,4,1,3,2,0:T(8,128)(2,1)S(1)}, u32[]{:S(2)}, u32[]{:S(2)}) async-start(bf16[32,2,1,1,16,512]{5,4,1,3,2,0:T(8,128)(2,1)} %copy.30), calls=%async_computation.4 | async-start | bytes 2097152 | tf_op jit(solution)/shard_map/all_to_all | solution.py:29
Sparse Core Ops, SparseCore 0:
  180.7 51.3 all-gather.1
where the time goes:
time: 450 us
  blocking collectives  213 us (47%)
  waiting for transfers between devices  156 us (35%)
  starting transfers between devices  23.4 us (5%)
  local copies, waits for them, and re-layouts  19.8 us (4%)
  between operations  13.6 us (3%)
  matrix products  13.4 us (3%)
  other arithmetic  10.5 us (2%)
    all_to_all x3, blocking collectives, turned_blocks(): whole = lax.all_to_all(whole, axes[k], k, k, tiled=True)  162 us
    all_to_all x1, waiting for transfers between devices, turned_blocks(): whole = lax.all_to_all(whole, axes[k], k, k, tiled=True)  104 us
    all_gather x1, waiting for transfers between devices, body(): received = lax.all_gather(received, 'tp', axis=2, tiled=True)  51.5 us
    all_to_all x1, blocking collectives, sent_and_summed(): lax.all_to_all(blocks, axis, split_axis=0, concat_axis=0, tiled=True)  51.3 us
    all_to_all x1, starting transfers between devices, turned_blocks(): whole = lax.all_to_all(whole, axes[k], k, k, tiled=True)  23.4 us
  transfers between devices with their start and end apart: 2, of which 2 were waited for; matrix products, arithmetic and copies ran while one was open for 0% of the time, Pallas kernels for 0%

commit v1 on v0

--- a/solution.py
+++ b/solution.py
@@ -9,6 +9,13 @@
 epsilon = 1e-06
 clamp_limit = 7.0
 swish_alpha = 1.702
+
+
+def compute_case(z, dim_k):
+    current_block = list(z.shape[1:])
+    current_block[dim_k] *= z.shape[0]
+    v1 = jnp.moveaxis(z, 0, dim_k).reshape(current_block)
+    return v1
 
 
 def cut_along(value, dim, devices):
@@ -73,7 +80,25 @@
     col_share = model_width // tp_count
     col_part = lax.dynamic_slice_in_dim(send_buffer, lax.axis_index("tp") * col_share, col_share, 2)
     received = exchange_by_chip(col_part, ("ep_0", "ep_1"), (1, 0), 0, 0)
-    received = lax.all_gather(received, "tp", axis=2, tiled=True)
+    n_peers_all = lax.axis_size("tp")
+    by_rank = [(u, (u + 1) % n_peers_all) for u in range(n_peers_all)]
+    parts_seen = [(it, h) for h, it in by_rank]
+    lower, block_next = ([], [])
+    for p in tuple(range(n_peers_all - 1)):
+        if p % 2 == 0:
+            outer = lax.ppermute(lower[-1] if lower else received, "tp", perm=by_rank)
+            lower.append(outer)
+        else:
+            outcome_arr = lax.ppermute(
+                block_next[-1] if block_next else received, axis_name="tp", perm=parts_seen
+            )
+            block_next.append(outcome_arr)
+    state_next = jnp.stack([*lower[::-1], received, *block_next])
+    z1 = lax.axis_index("tp")
+    inter = len(lower)
+    local_next = z1 - inter
+    state_next = state_next[(jnp.arange(n_peers_all) - local_next) % n_peers_all]
+    received = compute_case(state_next, 2)
     expert_rows = received.reshape(ep_count, local_experts, capacity, model_width)
     gate_pre = jnp.einsum("sjcd,jdf->sjcf", expert_rows, w_gate, preferred_element_type=jnp.float32)
     up_pre = jnp.einsum("sjcd,jdf->sjcf", expert_rows, w_up, preferred_element_type=jnp.float32)

time: 450 us -> 435 us (0.967)
  between operations: 13.6 us -> 0.27 us
  local copies, waits for them, and re-layouts: 19.8 us -> 29.6 us
  starting transfers between devices: 23.4 us -> 17.4 us
  waiting for transfers between devices: 156 us -> 150 us
    all_gather x1 -> x0, waiting for transfers between devices: 51.5 us -> none  [body(): received = lax.all_gather(received, 'tp', axis=2, tiled=True)]
    ppermute x0 -> x3, waiting for transfers between devices: none -> 45.3 us  [the longest x2 45.3 us: body(): outer = lax.ppermute(lower[-1] if lower else received, 'tp', perm=by_rank)]
    all_to_all x1, starting transfers between devices: 23.4 us -> 8.65 us  [turned_blocks(): whole = lax.all_to_all(whole, axes[k], k, k, tiled=True)]
    ppermute x0 -> x3, starting transfers between devices: none -> 8.71 us  [the longest x2 5.21 us: body(): outer = lax.ppermute(lower[-1] if lower else received, 'tp', perm=by_rank)]
    gather x0 -> x1, local copies, waits for them, and re-layouts: none -> 4.97 us  [body(): state_next[(jnp.arange(n_peers_all) - local_next) % n_peers_all]]
  transfers between devices with their start and end apart: 2 -> 4, of which waited for: 2 -> 3; matrix products, arithmetic and copies ran while one was open for 0% -> 0% of each run, Pallas kernels for 0% -> 0%
where the time goes in v1:
time: 435 us; the launch traced here: 434 us
  blocking collectives  213 us (49%)
  waiting for transfers between devices  150 us (34%)
  local copies, waits for them, and re-layouts  29.6 us (7%)
  starting transfers between devices  17.4 us (4%)
  other arithmetic  13.9 us (3%)
  matrix products  9.8 us (2%)
    all_to_all x3, blocking collectives, turned_blocks(): whole = lax.all_to_all(whole, axes[k], k, k, tiled=True)  163 us
    all_to_all x1, waiting for transfers between devices, turned_blocks(): whole = lax.all_to_all(whole, axes[k], k, k, tiled=True)  105 us
    all_to_all x1, blocking collectives, sent_and_summed(): lax.all_to_all(blocks, axis, split_axis=0, concat_axis=0, tiled=True)  49.9 us
    ppermute x2, waiting for transfers between devices, body(): outer = lax.ppermute(lower[-1] if lower else received, 'tp', perm=by_rank)  45.3 us
  transfers between devices with their start and end apart: 4, of which 3 were waited for; matrix products, arithmetic and copies ran while one was open for 0% of the time, Pallas kernels for 0%

profile of v1, /device:TPU:33, one launch (start us, length us, event | category | flops | bytes accessed | tf_op | source)
XLA Modules:
  0.0 433.9 jit_solution(7259692507942186997)
XLA Ops:
  0.0 0.0 copy-start
  0.0 0.9 copy.30
  0.9 0.1 eq.31
  1.0 0.1 eq.27
  1.1 0.7 broadcast_multiply_fusion
  1.8 1.8 reduce-window.6
  3.6 0.3 slice_reduce_fusion
  3.9 0.1 copy.29
  4.1 0.1 mul.68
  4.2 0.1 fusion.26
  4.3 3.4 scatter_custom_fusion
  7.7 1.4 fusion
  9.1 1.4 fusion.2
  10.5 0.1 concatenate.3
  10.6 6.0 %gather_fusion = bf16[1024,2048]{1,0:T(8,128)(2,1)} fusion(bf16[193,2048]{1,0:T(8,128)(2,1)S(1)} %concatenate.3, s32[1024]{0:T(1024)S(1)} %fusion.30), kind=kCustom, calls=%fused_computation | custom fusion | bytes 8392704 | tf_op jit(solution)/shard_map/gather | solution.py:79
  16.6 1.3 constant_dynamic-slice_fusion
  17.9 0.1 copy.33
  18.0 45.6 %all_to_all.25 = bf16[32,2,1,16,512]{4,3,0,2,1:T(8,128)(2,1)S(1)} all-to-all(bf16[32,2,1,16,512]{4,3,0,2,1:T(8,128)(2,1)S(1)} %copy.33), channel_id=1, replica_groups=mesh['grp'=2,'ep_0'=32,'ep_1'=2,'tp'=4] {'ep_1'}, dimensions={1} | all-to-all | bytes 2097152 | tf_op jit(solution)/shard_map/all_to_all | solution.py:36
  63.7 0.1 copy.34
  63.8 109.9 %all_to_all.26 = bf16[32,2,1,16,512]{4,3,1,2,0:T(8,128)(2,1)S(1)} all-to-all(bf16[32,2,1,16,512]{4,3,1,2,0:T(8,128)(2,1)S(1)} %copy.34), channel_id=1, replica_groups=mesh['grp'=2,'ep_0'=32,'ep_1'=2,'tp'=4] {'ep_0'}, dimensions={0} | all-to-all | bytes 2097152 | tf_op jit(solution)/shard_map/all_to_all | solution.py:36
  173.7 3.3 collective-permute-start
  177.0 3.5 collective-permute-start.2
  180.5 20.8 %collective-permute-done = bf16[64,16,512]{2,1,0:T(8,128)(2,1)S(1)} collective-permute-done((bf16[64,16,512]{2,1,0:T(8,128)(2,1)S(1)}, bf16[64,16,512]{2,1,0:T(8,128)(2,1)S(1)}, u32[]{:S(2)}, u32[]{:S(2)}) %collective-permute-start) | collective-permute-done | bytes 1048608 | tf_op jit(solution)/shard_map/ppermute | solution.py:89
  201.2 1.9 collective-permute-start.1
  203.2 0.0 collective-permute-done.2
  203.2 24.6 %collective-permute-done.1 = bf16[64,16,512]{2,1,0:T(8,128)(2,1)} collective-permute-done((bf16[64,16,512]{2,1,0:T(8,128)(2,1)S(1)}, bf16[64,16,512]{2,1,0:T(8,128)(2,1)}, u32[]{:S(2)}, u32[]{:S(2)}) %collective-permute-start.1) | collective-permute-done | bytes 1048608 | tf_op jit(solution)/shard_map/ppermute | solution.py:89
  227.8 3.4 pad_maximum_fusion
  231.2 5.0 %gather_fusion.1 = bf16[4,64,16,512]{3,2,1,0:T(8,128)(2,1)} fusion(bf16[4,64,16,512]{3,2,1,0:T(8,128)(2,1)} %pad_maximum_fusion, s32[1024]{0:T(1024)S(1)} %pad_clamp_fusion.1), kind=kCustom, calls=%fused_computation.1 | custom fusion | bytes 8388624 | tf_op jit(solution)/shard_map/gather | solution.py:100
  236.2 0.0 copy-start.3
  236.2 2.9 copy.42
  239.1 0.0 copy-start.1
  239.1 0.0 copy-start.4
  239.1 1.9 copy-done.1
  241.0 0.0 copy-done.3
  241.1 1.3 fusion.3
  242.3 0.0 copy-done
  242.3 0.0 copy-done.4
  242.3 8.6 %convolution_convert_fusion = bf16[64,16,2048]{2,1,0:T(8,128)(2,1)} fusion(bf16[64,16,2048]{2,1,0:T(8,128)(2,1)} %bitcast.91, bf16[1,256,2048]{2,1,0:T(8,128)(2,1)S(1)} %copy-done, bf16[1,2048,256]{2,1,0:T(8,128)(2,1)S(1)} %copy-done.4, f32[64,1,16,256]{3,2,0,1:T(8,128)S(1)} %fusion.3), kind=kOutput, calls=%fused_computation.6 | convolution fusion | flops 2151940096 | bytes 11534336 | tf_op jit(solution)/shard_map/sjcf,jfd->sjcd/dot_general | solution.py:108
  250.9 2.8 copy.45
  253.7 49.9 %all_to_all.27 = bf16[4,64,1,16,512]{4,3,1,2,0:T(8,128)(2,1)} all-to-all(bf16[4,64,1,16,512]{4,3,1,2,0:T(8,128)(2,1)S(1)} %bitcast.87), channel_id=1, replica_groups=mesh['grp'=2,'ep_0'=32,'ep_1'=2,'tp'=4] {'tp'}, dimensions={0} | all-to-all | bytes 8388608 | tf_op jit(solution)/shard_map/all_to_all | solution.py:48
  303.6 3.3 reduce_sum.44
  306.9 0.0 copy-start.2
  307.0 0.1 copy.37
  307.0 7.5 %all_to_all.28 = bf16[32,2,1,1,16,512]{5,4,0,3,2,1:T(8,128)(2,1)S(1)} all-to-all(bf16[32,2,1,1,16,512]{5,4,0,3,2,1:T(8,128)(2,1)S(1)} %copy.37), channel_id=1, replica_groups=mesh['grp'=2,'ep_0'=32,'ep_1'=2,'tp'=4] {'ep_1'}, dimensions={1} | all-to-all | bytes 2097152 | tf_op jit(solution)/shard_map/all_to_all | solution.py:36
  314.6 1.1 copy.38
  315.7 8.7 %all-to-all-start.4 = ((bf16[32,2,1,1,16,512]{5,4,1,3,2,0:T(8,128)(2,1)}), bf16[32,2,1,1,16,512]{5,4,1,3,2,0:T(8,128)(2,1)S(1)}, u32[]{:S(2)}, u32[]{:S(2)}) async-start(bf16[32,2,1,1,16,512]{5,4,1,3,2,0:T(8,128)(2,1)} %copy.38), calls=%async_computation.4 | async-start | bytes 2097152 | tf_op jit(solution)/shard_map/all_to_all | solution.py:36
  324.3 0.0 copy-done.2
  324.3 0.1 copy.39
  324.5 104.5 %all-to-all-done.4 = bf16[32,2,1,1,16,512]{5,4,1,3,2,0:T(8,128)(2,1)S(1)} async-done(((bf16[32,2,1,1,16,512]{5,4,1,3,2,0:T(8,128)(2,1)}), bf16[32,2,1,1,16,512]{5,4,1,3,2,0:T(8,128)(2,1)S(1)}, u32[]{:S(2)}, u32[]{:S(2)}) %all-to-all-start.4) | async-done | bytes 1048608 | tf_op jit(solution)/shard_map/all_to_all | solution.py:36
  429.0 2.7 gather_fusion.2
  431.7 0.5 reshape.153
  432.2 1.7 multiply_reduce_fusion
  (9 shorter events, 0.1 us)
Async XLA Ops:
  0.0 242.3 %copy-start = (bf16[1,256,2048]{2,1,0:T(8,128)(2,1)S(1)}, bf16[1,256,2048]{2,1,0:T(8,128)(2,1)}, u32[]{:S(2)}) copy-start(bf16[1,256,2048]{2,1,0:T(8,128)(2,1)} %param.11) | copy-start | bytes 3145732
  173.7 27.5 %collective-permute-start = (bf16[64,16,512]{2,1,0:T(8,128)(2,1)S(1)}, bf16[64,16,512]{2,1,0:T(8,128)(2,1)S(1)}, u32[]{:S(2)}, u32[]{:S(2)}) collective-permute-start(bf16[64,16,512]{2,1,0:T(8,128)(2,1)S(1)} %bitcast.94), channel_id=1, source_target_pairs={{0,1},{1,2},{2,3},{3,0},{4,5},{5,6},{6,7},{7,4},{8,9},{9,10},{10,1... | collective-permute-start | bytes 3145736 | tf_op jit(solution)/shard_map/ppermute | solution.py:89
  177.0 26.2 %collective-permute-start.2 = (bf16[64,16,512]{2,1,0:T(8,128)(2,1)S(1)}, bf16[64,16,512]{2,1,0:T(8,128)(2,1)}, u32[]{:S(2)}, u32[]{:S(2)}) collective-permute-start(bf16[64,16,512]{2,1,0:T(8,128)(2,1)S(1)} %bitcast.95), channel_id=1, source_target_pairs={{1,0},{2,1},{3,2},{0,3},{5,4},{6,5},{7,6},{4,7},{9,8},{10,9},{11,1... | collective-permute-start | bytes 3145736 | tf_op jit(solution)/shard_map/ppermute | solution.py:92
  201.2 26.6 %collective-permute-start.1 = (bf16[64,16,512]{2,1,0:T(8,128)(2,1)S(1)}, bf16[64,16,512]{2,1,0:T(8,128)(2,1)}, u32[]{:S(2)}, u32[]{:S(2)}) collective-permute-start(bf16[64,16,512]{2,1,0:T(8,128)(2,1)S(1)} %collective-permute-done), channel_id=1, source_target_pairs={{0,1},{1,2},{2,3},{3,0},{4,5},{5,6},{6,7},{7,4},{8,9},{9,10},{10,1... | collective-permute-start | bytes 3145736 | tf_op jit(solution)/shard_map/ppermute | solution.py:89
  236.2 4.9 %copy-start.3 = (bf16[1,2048,256]{2,1,0:T(8,128)(2,1)S(1)}, bf16[1,2048,256]{2,1,0:T(8,128)(2,1)}, u32[]{:S(2)}) copy-start(bf16[1,2048,256]{2,1,0:T(8,128)(2,1)} %param.9) | copy-start | bytes 3145732
  239.1 1.9 copy-start.1
  239.1 3.2 copy-start.4
  306.9 17.4 %copy-start.2 = (f32[192,4]{0,1:T(4,128)S(1)}, f32[192,4]{0,1:T(4,128)}, u32[]{:S(2)}) copy-start(f32[192,4]{0,1:T(4,128)} %param.13) | copy-start | bytes 9220
  315.7 113.3 %all-to-all-start.4 = ((bf16[32,2,1,1,16,512]{5,4,1,3,2,0:T(8,128)(2,1)}), bf16[32,2,1,1,16,512]{5,4,1,3,2,0:T(8,128)(2,1)S(1)}, u32[]{:S(2)}, u32[]{:S(2)}) async-start(bf16[32,2,1,1,16,512]{5,4,1,3,2,0:T(8,128)(2,1)} %copy.38), calls=%async_computation.4 | async-start | bytes 2097152 | tf_op jit(solution)/shard_map/all_to_all | solution.py:36
